TPU v7x, 768 devices: a whole 4x8x12 slice. The times are simulated.
768 devices in a mesh: gr: 3 (over z_hi), sp: 32 (over z_lo, y), tp: 8 (over x, core).
Axes of the slice: x: 4, y: 8, z: 12 (z_hi: 3, z_lo: 4; z = z_hi * 4 + z_lo), core: 2. Of those that a mesh axis runs over, the one named last changes fastest.
Arguments:
- tokens: bfloat16 [6, 16384, 4096], P('gr', ('sp', 'tp')), parts along dimension 0, may hold values from -6 to 6
- norm_gain: bfloat16 [4096], replicated, may hold values from 0.099609375 to 1.8984375
- key_weight: bfloat16 [4096, 1024], P(None, 'tp'), may hold values from -0.09375 to 0.09375
- value_weight: bfloat16 [4096, 1024], P(None, 'tp'), may hold values from -0.09375 to 0.09375
- cum_gates: float32 [6, 16384, 16], P('gr', 'sp', 'tp'), parts along dimension 0, may hold values from -2733 to 0, as said below
- new_query: bfloat16 [6, 1024], P('gr', 'tp'), parts along dimension 0, may hold values from -240 to 240
- new_key: bfloat16 [6, 1024], P('gr', 'tp'), parts along dimension 0, may hold values from -6 to 6
- new_value: bfloat16 [6, 1024], P('gr', 'tp'), parts along dimension 0, may hold values from -6 to 6
- new_gate: float32 [6, 16], P('gr', 'tp'), parts along dimension 0, may hold values from -5 to -1.5
Outputs:
- key_cache: bfloat16 [6, 16384, 1024], P('gr', 'sp', 'tp'), parts along dimension 0
- value_cache: bfloat16 [6, 16384, 1024], P('gr', 'sp', 'tp'), parts along dimension 0
- readout: bfloat16 [6, 1024], P('gr', 'tp'), parts along dimension 0
There are 3 independent parts, one for each index of `gr`. A program takes and returns all parts, laid end to end along the dimension named above; an argument that names none is the same for every part. Nothing has to cross between parts.
Inputs may be any that keep to these rules, and one draw needn't show every extreme that they name: `cum_gates`: along positions, for each prompt and head, the values never rise.
All inputs are finite; a program needn't handle non-finite values.
Results may differ from a plain program's by a relative error of at most 0.005.
The roundings to bfloat16 on the way count: a program that leaves them out, or rounds other values in their place, can miss the bound.
Values may be sent and summed in bfloat16 or wider, within the bound.
No kernel may reach another device: no remote copies, remote signals or barrier semaphores. Data moves between devices by JAX's collectives and lax.ppermute only.
A program may use at most 64 MiB of HBM per device.

v0:
```python
import functools

import jax
import jax.numpy as jnp
from jax import lax
from jax.experimental import pallas as pl
from jax.experimental.pallas import tpu as pltpu
from jax.sharding import PartitionSpec as P


HD = 64
EPS = 1e-06
MASKED = -1e30


VMEM = pl.BlockSpec(memory_space=pltpu.VMEM)

EARLY = ((0, 0), (0, 1), (3, 0), (1, 1), (1, 0), (3, 1))
LATE = ((2, 0), (2, 1))


def project_kernel(count, *refs):
    xs, (gain, wo, wp, own, par, n_s) = refs[:count], refs[count:]
    half, width = xs[0].shape
    step = 16

    def normalize(x, base):
        def rows_of(i, carry):
            rows = pl.ds(pl.multiple_of(i * step, step), step)
            total = jnp.zeros((step, 128), jnp.float32)
            for c in range(width // 1024):
                part = x[rows, pl.ds(c * 1024, 1024)].astype(jnp.float32)
                part = part * part
                for j in range(8):
                    total = total + part[:, j * 128 : (j + 1) * 128]
            mean = jnp.sum(total, axis=-1, keepdims=True) * (1.0 / width)
            scale = lax.rsqrt(mean + EPS)
            out = pl.ds(pl.multiple_of(base + i * step, step), step)
            for c in range(width // 1024):
                at = pl.ds(c * 1024, 1024)
                part = x[rows, at].astype(jnp.float32)
                part = part * scale * gain[:, at].astype(jnp.float32)
                n_s[out, at] = part.astype(jnp.bfloat16)
            return carry

        lax.fori_loop(0, half // step, rows_of, 0, unroll=2)

    for k, x in enumerate(xs):
        normalize(x, k * half)
    for w, out in ((wo, own), (wp, par)):
        acc = jnp.dot(n_s[...], w[...], preferred_element_type=jnp.float32)
        out[...] = acc.astype(jnp.bfloat16).reshape(out.shape)


def project(xs, gain, wo, wp):
    count = len(xs)
    half, width = xs[0].shape
    cols = wo.shape[1]
    out = jax.ShapeDtypeStruct((count, half, cols), jnp.bfloat16)
    return pl.pallas_call(
        functools.partial(project_kernel, count),
        out_shape=(out, out),
        in_specs=[VMEM] * (count + 3),
        out_specs=(VMEM, VMEM),
        scratch_shapes=[pltpu.VMEM((count * half, width), jnp.bfloat16)],
        compiler_params=pltpu.CompilerParams(vmem_limit_bytes=24 * 1024 * 1024),
        cost_estimate=pl.CostEstimate(
            flops=2 * count * half * width * 2 * cols,
            bytes_accessed=6 * 1024 * 1024,
            transcendentals=0,
        ),
        name="project",
    )(*xs, gain, wo, wp)


def prepare_kernel(cum, q, fk, fv, ng, gates, qm, small):
    block, cols = gates.shape[1:]
    shape = (cols, cols)
    same = lax.broadcasted_iota(jnp.int32, shape, 0) // HD == (
        lax.broadcasted_iota(jnp.int32, shape, 1) // HD
    )
    first = lax.broadcasted_iota(jnp.int32, (2, cols), 1) < HD
    for p in range(2):
        spread = [jnp.broadcast_to(cum[p, h : h + 1, :], (HD, block)) for h in range(2)]
        gates[p] = jnp.concatenate(spread, axis=0).T
        down = jnp.broadcast_to(q[p : p + 1, :].astype(jnp.float32), shape).T
        qm[p] = jnp.where(same, down, 0.0).astype(jnp.bfloat16)
        fresh = jnp.dot(fk[...], qm[p], preferred_element_type=jnp.float32)
        small[p : p + 1, :] = fresh[p : p + 1] * (HD**-0.5)
    small[2:4, :] = fv[...].astype(jnp.float32)
    small[4:6, :] = jnp.where(first, ng[:, 0:1], ng[:, 1:2])
    small[6:8, :] = jnp.zeros((2, cols), jnp.float32)


def prepare(cum, q, fk, fv, ng):
    block, cols = cum.shape[2], q.shape[1]
    return pl.pallas_call(
        prepare_kernel,
        out_shape=(
            jax.ShapeDtypeStruct((2, block, cols), jnp.float32),
            jax.ShapeDtypeStruct((2, cols, cols), jnp.bfloat16),
            jax.ShapeDtypeStruct((8, cols), jnp.float32),
        ),
        in_specs=[VMEM] * 5,
        out_specs=(VMEM,) * 3,
        compiler_params=pltpu.CompilerParams(vmem_limit_bytes=8 * 1024 * 1024),
        cost_estimate=pl.CostEstimate(
            flops=1024 * 1024, bytes_accessed=1024 * 1024, transcendentals=0
        ),
        name="prepare",
    )(cum, q, fk, fv, ng)


def attend_kernel(own1, own2, got1, got2, gates, qm, small, keys, values, part):
    tp = lax.axis_index("tp")
    x, core = tp // 2, lax.rem(tp, 2)
    half = own1.shape[1]
    members, _, cols = part.shape
    block = keys.shape[1]
    for side, refs in enumerate(((own1, own2), (got1, got2))):
        which = lax.rem(core + side, 2)
        for ref, places in zip(refs, (EARLY, LATE)):
            for k, (off, p) in enumerate(places):
                at = pl.multiple_of((lax.rem(x + off, 4) * 2 + which) * half, half)
                keys[p, pl.ds(at, half), :] = ref[k, :, :cols]
                values[p, pl.ds(at, half), :] = ref[k, :, cols:]
    last = lax.axis_index("sp") == lax.axis_size("sp") - 1
    s0, fv, fg = small[0:2, :], small[2:4, :], small[4:6, :]
    for p in range(2):
        one = slice(p, p + 1)
        scores = jnp.dot(keys[p], qm[p], preferred_element_type=jnp.float32)
        scores = scores * (HD**-0.5) - gates[p]
        fresh = s0[one] - (gates[p, block - 1 : block, :] + fg[one])
        fresh = jnp.where(last, fresh, MASKED)
        top = jnp.maximum(jnp.max(scores, axis=0, keepdims=True), fresh)
        weights = jnp.exp(scores - top)
        fresh_weight = jnp.exp(fresh - top)
        total = jnp.sum(weights, axis=0, keepdims=True) + fresh_weight
        acc = jnp.sum(weights * values[p].astype(jnp.float32), axis=0, keepdims=True)
        acc = acc + fresh_weight * fv[one]
        for r, row in ((2 * p, top), (2 * p + 1, top), (2 * p + 4, total), (2 * p + 5, acc)):
            part[:, r : r + 1, :] = jnp.broadcast_to(row[None], (members, 1, cols))


def attend(own1, own2, got1, got2, gates, qm, small, members):
    block, cols = gates.shape[1:]
    cache = jax.ShapeDtypeStruct((2, block, cols), jnp.bfloat16)
    return pl.pallas_call(
        attend_kernel,
        out_shape=(cache, cache, jax.ShapeDtypeStruct((members, 8, cols), jnp.float32)),
        in_specs=[VMEM] * 7,
        out_specs=(VMEM, VMEM, VMEM),
        compiler_params=pltpu.CompilerParams(vmem_limit_bytes=16 * 1024 * 1024),
        cost_estimate=pl.CostEstimate(
            flops=64 * 1024 * 1024, bytes_accessed=2 * 1024 * 1024, transcendentals=0
        ),
        name="attend",
    )(own1, own2, got1, got2, gates, qm, small)


def merge_kernel(parts, out):
    tops = parts[:, 0:4, :]
    scale = jnp.exp(tops - jnp.max(tops, axis=0, keepdims=True))
    sums = jnp.sum(scale * parts[:, 4:8, :], axis=0)
    for p in range(2):
        out[p : p + 1, :] = (
            sums[2 * p + 1 : 2 * p + 2] / sums[2 * p : 2 * p + 1]
        ).astype(jnp.bfloat16)


def merge(parts):
    cols = parts.shape[2]
    return pl.pallas_call(
        merge_kernel,
        out_shape=jax.ShapeDtypeStruct((2, cols), jnp.bfloat16),
        in_specs=[VMEM],
        out_specs=VMEM,
        name="merge",
    )(parts)


def shift(x, by):
    return lax.ppermute(x, "tp", by)


def body(
    tokens, norm_gain, key_weight, value_weight, cum_gates, new_query, new_key, new_value, new_gate
):
    members = lax.axis_size("sp")
    tps = lax.axis_size("tp")
    right = [(i, (i + 2) % tps) for i in range(tps)]
    left = [(i, (i - 2) % tps) for i in range(tps)]
    swap = [(i, i ^ 1) for i in range(tps)]
    gain = norm_gain.reshape(1, -1)
    a0, b0 = tokens[0], tokens[1]
    a_l = shift(a0, right)
    b_r = shift(b0, left)
    b_l = shift(b0, right)
    a_r = shift(a0, left)
    a_2 = shift(a_l, right)
    b_2 = shift(b_r, left)
    wo = jnp.concatenate([key_weight, value_weight], axis=1)
    wp = shift(wo, swap)

    made = prepare(
        jnp.swapaxes(cum_gates, 1, 2), new_query, new_key, new_value, new_gate
    )
    gain, wp, made = lax.optimization_barrier((gain, wp, made))
    gates, qm, small = made

    own1, par1 = project((a0, b0, a_l, b_r, a_r, b_l), gain, wo, wp)
    got1 = shift(par1, swap)
    own2, par2 = project((a_2, b_2), gain, wo, wp)
    got2 = shift(par2, swap)
    keys, values, part = attend(own1, own2, got1, got2, gates, qm, small, members)
    parts = lax.all_to_all(part, "sp", split_axis=0, concat_axis=0, tiled=True)
    return keys, values, merge(parts)


def solution(mesh):
    in_specs = (
        P("gr", ("sp", "tp"), None),
        P(),
        P(None, "tp"),
        P(None, "tp"),
        P("gr", "sp", "tp"),
        P("gr", "tp"),
        P("gr", "tp"),
        P("gr", "tp"),
        P("gr", "tp"),
    )
    out_specs = (P("gr", "sp", "tp"), P("gr", "sp", "tp"), P("gr", "tp"))
    return jax.shard_map(body, mesh=mesh, in_specs=in_specs, out_specs=out_specs, check_vma=False)
```

profile of v0, /device:TPU:1, one launch (start us, length us, event | category | flops | bytes accessed | tf_op | source)
XLA Modules:
  0.0 76.6 jit_solution(14453063816972513647)
XLA Ops:
  0.6 0.0 copy-start.5
  0.6 0.0 copy-start.6
  0.7 1.6 %constant_dynamic-update-slice_fusion.1 = bf16[4096,256]{1,0:T(8,128)(2,1)S(1)} fusion(bf16[4096,128]{1,0:T(8,128)(2,1)} %param.11), kind=kLoop, calls=%fused_computation.3 | loop fusion | bytes 2097152
  2.2 0.0 copy-done.5
  2.2 0.0 copy-start.7
  2.2 0.0 copy-start
  2.2 0.0 copy-start.1
  2.3 0.0 copy-start.2
  2.3 0.0 copy-start.3
  2.3 0.0 copy-start.4
  2.3 0.2 constant_dynamic-update-slice_fusion.refs_7_.refs_3_
  2.5 12.4 %collective-permute-start.4 = (bf16[4096,256]{1,0:T(8,128)(2,1)S(1)}, bf16[4096,256]{1,0:T(8,128)(2,1)S(1)}, u32[]{:S(2)}, u32[]{:S(2)}) collective-permute-start(bf16[4096,256]{1,0:T(8,128)(2,1)S(1)} %constant_dynamic-update-slice_fusion.refs_7_.refs_3_), channel_id=1, source_target_pairs={{0,1},{1,0},{2,3},{3,2},{4,5},{5,4},{6,7},{7,6},{8,9},{9,8},{10,11... | collective-permute-start | bytes 6291464 | tf_op jit(solution)/shard_map/ppermute | solution.py:183
  14.9 0.0 copy-done.6
  14.9 0.1 slice_bitcast_fusion
  15.0 1.9 %collective-permute-start = (bf16[64,4096]{1,0:T(8,128)(2,1)S(1)}, bf16[64,4096]{1,0:T(8,128)(2,1)S(1)}, u32[]{:S(2)}, u32[]{:S(2)}) collective-permute-start(bf16[64,4096]{1,0:T(8,128)(2,1)S(1)} %get-tuple-element.34.refs_0_), channel_id=1, source_target_pairs={{0,2},{1,3},{2,4},{3,5},{4,6},{5,7},{6,0},{7,1},{8,10},{9,11},{10,... | collective-permute-start | bytes 1572872 | tf_op jit(solution)/shard_map/ppermute | solution.py:183
  17.0 4.6 %collective-permute-start.1 = (bf16[64,4096]{1,0:T(8,128)(2,1)S(1)}, bf16[64,4096]{1,0:T(8,128)(2,1)S(1)}, u32[]{:S(2)}, u32[]{:S(2)}) collective-permute-start(bf16[64,4096]{1,0:T(8,128)(2,1)S(1)} %get-tuple-element.33.refs_1_), channel_id=1, source_target_pairs={{0,6},{1,7},{2,0},{3,1},{4,2},{5,3},{6,4},{7,5},{8,14},{9,15},{10,... | collective-permute-start | bytes 1572872 | tf_op jit(solution)/shard_map/ppermute | solution.py:183
  21.5 1.9 %collective-permute-start.2 = (bf16[64,4096]{1,0:T(8,128)(2,1)S(1)}, bf16[64,4096]{1,0:T(8,128)(2,1)S(1)}, u32[]{:S(2)}, u32[]{:S(2)}) collective-permute-start(bf16[64,4096]{1,0:T(8,128)(2,1)S(1)} %get-tuple-element.34.refs_0_), channel_id=1, source_target_pairs={{0,6},{1,7},{2,0},{3,1},{4,2},{5,3},{6,4},{7,5},{8,14},{9,15},{10,... | collective-permute-start | bytes 1572872 | tf_op jit(solution)/shard_map/ppermute | solution.py:183
  23.5 3.4 %collective-permute-start.3 = (bf16[64,4096]{1,0:T(8,128)(2,1)S(1)}, bf16[64,4096]{1,0:T(8,128)(2,1)S(1)}, u32[]{:S(2)}, u32[]{:S(2)}) collective-permute-start(bf16[64,4096]{1,0:T(8,128)(2,1)S(1)} %get-tuple-element.33.refs_1_), channel_id=1, source_target_pairs={{0,2},{1,3},{2,4},{3,5},{4,6},{5,7},{6,0},{7,1},{8,10},{9,11},{10,... | collective-permute-start | bytes 1572872 | tf_op jit(solution)/shard_map/ppermute | solution.py:183
  26.8 4.8 %collective-permute-done.refs_2_ = bf16[64,4096]{1,0:T(8,128)(2,1)S(1)} collective-permute-done((bf16[64,4096]{1,0:T(8,128)(2,1)S(1)}, bf16[64,4096]{1,0:T(8,128)(2,1)S(1)}, u32[]{:S(2)}, u32[]{:S(2)}) %collective-permute-start) | collective-permute-done | bytes 524320 | tf_op jit(solution)/shard_map/ppermute | solution.py:183
  31.6 1.9 %collective-permute-start.5 = (bf16[64,4096]{1,0:T(8,128)(2,1)S(1)}, bf16[64,4096]{1,0:T(8,128)(2,1)S(1)}, u32[]{:S(2)}, u32[]{:S(2)}) collective-permute-start(bf16[64,4096]{1,0:T(8,128)(2,1)S(1)} %collective-permute-done.refs_2_), channel_id=1, source_target_pairs={{0,2},{1,3},{2,4},{3,5},{4,6},{5,7},{6,0},{7,1},{8,10},{9,11},{10,... | collective-permute-start | bytes 1572872 | tf_op jit(solution)/shard_map/ppermute | solution.py:183
  33.5 0.0 collective-permute-done.1.refs_3_
  33.5 4.6 %collective-permute-start.6 = (bf16[64,4096]{1,0:T(8,128)(2,1)S(1)}, bf16[64,4096]{1,0:T(8,128)(2,1)S(1)}, u32[]{:S(2)}, u32[]{:S(2)}) collective-permute-start(bf16[64,4096]{1,0:T(8,128)(2,1)S(1)} %collective-permute-done.1.refs_3_), channel_id=1, source_target_pairs={{0,6},{1,7},{2,0},{3,1},{4,2},{5,3},{6,4},{7,5},{8,14},{9,15},{10,... | collective-permute-start | bytes 1572872 | tf_op jit(solution)/shard_map/ppermute | solution.py:183
  38.1 0.0 copy-done.7
  38.1 0.0 copy-done
  38.2 0.0 copy-done.1
  38.2 0.0 copy-done.2
  38.2 0.0 copy-done.3
  38.2 0.0 copy-done.4
  38.2 0.3 prepare.1
  38.5 0.0 collective-permute-done.4.refs_8_.refs_4_
  38.5 5.3 %collective-permute-done.2.refs_4_ = bf16[64,4096]{1,0:T(8,128)(2,1)S(1)} collective-permute-done((bf16[64,4096]{1,0:T(8,128)(2,1)S(1)}, bf16[64,4096]{1,0:T(8,128)(2,1)S(1)}, u32[]{:S(2)}, u32[]{:S(2)}) %collective-permute-start.2) | collective-permute-done | bytes 524320 | tf_op jit(solution)/shard_map/ppermute | solution.py:183
  43.7 0.0 collective-permute-done.3.refs_5_
  43.8 3.9 %project.2 = (bf16[6,64,256]{2,1,0:T(8,128)(2,1)S(1)}, bf16[6,64,256]{2,1,0:T(8,128)(2,1)S(1)}) custom-call(bf16[64,4096]{1,0:T(8,128)(2,1)S(1)} %get-tuple-element.34.refs_0_, bf16[64,4096]{1,0:T(8,128)(2,1)S(1)} %get-tuple-element.33.refs_1_, bf16[64,4096]{1,0:T(8,128)(2,1)S(1)} %collective-permute-done.refs_2_, ...), custom_call_target="tpu_custom_call" | custom-call | flops 1610612736 | bytes 6291456 | tf_op jit(solution)/shard_map/project/pallas_call | solution.py:60
  47.7 3.8 %collective-permute-start.7 = (bf16[6,64,256]{2,1,0:T(8,128)(2,1)S(1)}, bf16[6,64,256]{2,1,0:T(8,128)(2,1)S(1)}, u32[]{:S(2)}, u32[]{:S(2)}) collective-permute-start(bf16[6,64,256]{2,1,0:T(8,128)(2,1)S(1)} %get-tuple-element.25), channel_id=1, source_target_pairs={{0,1},{1,0},{2,3},{3,2},{4,5},{5,4},{6,7},{7,6},{8,9},{9,8},{10,11... | collective-permute-start | bytes 589832 | tf_op jit(solution)/shard_map/ppermute | solution.py:183
  51.5 2.6 %collective-permute-done.5.refs_0_ = bf16[64,4096]{1,0:T(8,128)(2,1)S(1)} collective-permute-done((bf16[64,4096]{1,0:T(8,128)(2,1)S(1)}, bf16[64,4096]{1,0:T(8,128)(2,1)S(1)}, u32[]{:S(2)}, u32[]{:S(2)}) %collective-permute-start.5) | collective-permute-done | bytes 524320 | tf_op jit(solution)/shard_map/ppermute | solution.py:183
  54.1 0.9 %collective-permute-done.6.refs_1_ = bf16[64,4096]{1,0:T(8,128)(2,1)S(1)} collective-permute-done((bf16[64,4096]{1,0:T(8,128)(2,1)S(1)}, bf16[64,4096]{1,0:T(8,128)(2,1)S(1)}, u32[]{:S(2)}, u32[]{:S(2)}) %collective-permute-start.6) | collective-permute-done | bytes 524320 | tf_op jit(solution)/shard_map/ppermute | solution.py:183
  55.0 1.4 %project.3 = (bf16[2,64,256]{2,1,0:T(8,128)(2,1)S(1)}, bf16[2,64,256]{2,1,0:T(8,128)(2,1)S(1)}) custom-call(bf16[64,4096]{1,0:T(8,128)(2,1)S(1)} %collective-permute-done.5.refs_0_, bf16[64,4096]{1,0:T(8,128)(2,1)S(1)} %collective-permute-done.6.refs_1_, bf16[1,4096]{1,0:T(2,128)(2,1)S(1)} %reshape.9.refs_6_.refs_2_, ...), custom_call_target="tpu_custom_call" | custom-call | flops 536870912 | bytes 6291456 | tf_op jit(solution)/shard_map/project/pallas_call | solution.py:60
  56.4 3.1 %collective-permute-start.8 = (bf16[2,64,256]{2,1,0:T(8,128)(2,1)S(1)}, bf16[2,64,256]{2,1,0:T(8,128)(2,1)S(1)}, u32[]{:S(2)}, u32[]{:S(2)}) collective-permute-start(bf16[2,64,256]{2,1,0:T(8,128)(2,1)S(1)} %get-tuple-element.26), channel_id=1, source_target_pairs={{0,1},{1,0},{2,3},{3,2},{4,5},{5,4},{6,7},{7,6},{8,9},{9,8},{10,11... | collective-permute-start | bytes 196616 | tf_op jit(solution)/shard_map/ppermute | solution.py:183
  59.5 0.9 %collective-permute-done.8.got2 = bf16[2,64,256]{2,1,0:T(8,128)(2,1)S(1)} collective-permute-done((bf16[2,64,256]{2,1,0:T(8,128)(2,1)S(1)}, bf16[2,64,256]{2,1,0:T(8,128)(2,1)S(1)}, u32[]{:S(2)}, u32[]{:S(2)}) %collective-permute-start.8) | collective-permute-done | bytes 65568 | tf_op jit(solution)/shard_map/ppermute | solution.py:183
  60.4 0.0 collective-permute-done.7.got1
  60.4 1.1 %attend.1 = (bf16[2,512,128]{2,1,0:T(8,128)(2,1)}, bf16[2,512,128]{2,1,0:T(8,128)(2,1)}, f32[32,8,128]{2,1,0:T(8,128)S(1)}) custom-call(bf16[6,64,256]{2,1,0:T(8,128)(2,1)S(1)} %get-tuple-element.23.own1, bf16[2,64,256]{2,1,0:T(8,128)(2,1)S(1)} %get-tuple-element.24.own2, bf16[6,64,256]{2,1,0:T(8,128)(2,1)S(1)} %collective-permute-done.7.got1, ...), custom_call_target="tpu_custom_call" | custom-call | flops 67108864 | bytes 2097152 | tf_op jit(solution)/shard_map/attend/pallas_call | solution.py:148
  61.4 13.7 %all_to_all.5.parts = f32[32,8,128]{2,1,0:T(8,128)} all-to-all(f32[32,8,128]{2,1,0:T(8,128)S(1)} %get-tuple-element.32), channel_id=1, replica_groups=mesh['gr'=3,'sp'=32,'tp'=8] {'sp'}, dimensions={0} | all-to-all | bytes 262144 | tf_op jit(solution)/shard_map/all_to_all | solution.py:216
  75.1 1.5 %merge.1 = bf16[2,128]{1,0:T(2,128)(2,1)} custom-call(f32[32,8,128]{2,1,0:T(8,128)} %all_to_all.5.parts), custom_call_target="tpu_custom_call" | custom-call | tf_op jit(solution)/shard_map/merge/pallas_call | solution.py:173
  (1 shorter events, 0.0 us)
Async XLA Ops:
  0.6 1.6 %copy-start.5 = (bf16[4096,128]{1,0:T(8,128)(2,1)S(1)}, bf16[4096,128]{1,0:T(8,128)(2,1)}, u32[]{:S(2)}) copy-start(bf16[4096,128]{1,0:T(8,128)(2,1)} %param.12) | copy-start | bytes 3145732
  0.6 14.3 %copy-start.6 = (bf16[2,64,4096]{2,1,0:T(8,128)(2,1)S(1)}, bf16[2,64,4096]{2,1,0:T(8,128)(2,1)}, u32[]{:S(2)}) copy-start(bf16[2,64,4096]{2,1,0:T(8,128)(2,1)} %param.9) | copy-start | bytes 3145732
  2.2 35.9 %copy-start.7 = (bf16[4096]{0:T(1024)(128)(2,1)S(1)}, bf16[4096]{0:T(1024)(128)(2,1)}, u32[]{:S(2)}) copy-start(bf16[4096]{0:T(1024)(128)(2,1)} %param.10) | copy-start | bytes 24580
  2.2 35.9 %copy-start = (f32[2,512,2]{1,2,0:T(2,128)S(1)}, f32[2,512,2]{1,2,0:T(2,128)}, u32[]{:S(2)}) copy-start(f32[2,512,2]{1,2,0:T(2,128)} %param.13) | copy-start | bytes 24580
  2.2 35.9 %copy-start.1 = (f32[2,2]{1,0:T(2,128)S(1)}, f32[2,2]{1,0:T(2,128)}, u32[]{:S(2)}) copy-start(f32[2,2]{1,0:T(2,128)} %ng.1) | copy-start | bytes 52
  2.3 35.9 %copy-start.2 = (bf16[2,128]{1,0:T(2,128)(2,1)S(1)}, bf16[2,128]{1,0:T(2,128)(2,1)}, u32[]{:S(2)}) copy-start(bf16[2,128]{1,0:T(2,128)(2,1)} %q.1) | copy-start | bytes 1540
  2.3 35.9 %copy-start.3 = (bf16[2,128]{1,0:T(2,128)(2,1)S(1)}, bf16[2,128]{1,0:T(2,128)(2,1)}, u32[]{:S(2)}) copy-start(bf16[2,128]{1,0:T(2,128)(2,1)} %fk.1) | copy-start | bytes 1540
  2.3 35.9 %copy-start.4 = (bf16[2,128]{1,0:T(2,128)(2,1)S(1)}, bf16[2,128]{1,0:T(2,128)(2,1)}, u32[]{:S(2)}) copy-start(bf16[2,128]{1,0:T(2,128)(2,1)} %fv.1) | copy-start | bytes 1540
  2.5 35.9 %collective-permute-start.4 = (bf16[4096,256]{1,0:T(8,128)(2,1)S(1)}, bf16[4096,256]{1,0:T(8,128)(2,1)S(1)}, u32[]{:S(2)}, u32[]{:S(2)}) collective-permute-start(bf16[4096,256]{1,0:T(8,128)(2,1)S(1)} %constant_dynamic-update-slice_fusion.refs_7_.refs_3_), channel_id=1, source_target_pairs={{0,1},{1,0},{2,3},{3,2},{4,5},{5,4},{6,7},{7,6},{8,9},{9,8},{10,11... | collective-permute-start | bytes 6291464 | tf_op jit(solution)/shard_map/ppermute | solution.py:183
  15.0 16.6 %collective-permute-start = (bf16[64,4096]{1,0:T(8,128)(2,1)S(1)}, bf16[64,4096]{1,0:T(8,128)(2,1)S(1)}, u32[]{:S(2)}, u32[]{:S(2)}) collective-permute-start(bf16[64,4096]{1,0:T(8,128)(2,1)S(1)} %get-tuple-element.34.refs_0_), channel_id=1, source_target_pairs={{0,2},{1,3},{2,4},{3,5},{4,6},{5,7},{6,0},{7,1},{8,10},{9,11},{10,... | collective-permute-start | bytes 1572872 | tf_op jit(solution)/shard_map/ppermute | solution.py:183
  17.0 16.6 %collective-permute-start.1 = (bf16[64,4096]{1,0:T(8,128)(2,1)S(1)}, bf16[64,4096]{1,0:T(8,128)(2,1)S(1)}, u32[]{:S(2)}, u32[]{:S(2)}) collective-permute-start(bf16[64,4096]{1,0:T(8,128)(2,1)S(1)} %get-tuple-element.33.refs_1_), channel_id=1, source_target_pairs={{0,6},{1,7},{2,0},{3,1},{4,2},{5,3},{6,4},{7,5},{8,14},{9,15},{10,... | collective-permute-start | bytes 1572872 | tf_op jit(solution)/shard_map/ppermute | solution.py:183
  21.5 22.2 %collective-permute-start.2 = (bf16[64,4096]{1,0:T(8,128)(2,1)S(1)}, bf16[64,4096]{1,0:T(8,128)(2,1)S(1)}, u32[]{:S(2)}, u32[]{:S(2)}) collective-permute-start(bf16[64,4096]{1,0:T(8,128)(2,1)S(1)} %get-tuple-element.34.refs_0_), channel_id=1, source_target_pairs={{0,6},{1,7},{2,0},{3,1},{4,2},{5,3},{6,4},{7,5},{8,14},{9,15},{10,... | collective-permute-start | bytes 1572872 | tf_op jit(solution)/shard_map/ppermute | solution.py:183
  23.5 20.3 %collective-permute-start.3 = (bf16[64,4096]{1,0:T(8,128)(2,1)S(1)}, bf16[64,4096]{1,0:T(8,128)(2,1)S(1)}, u32[]{:S(2)}, u32[]{:S(2)}) collective-permute-start(bf16[64,4096]{1,0:T(8,128)(2,1)S(1)} %get-tuple-element.33.refs_1_), channel_id=1, source_target_pairs={{0,2},{1,3},{2,4},{3,5},{4,6},{5,7},{6,0},{7,1},{8,10},{9,11},{10,... | collective-permute-start | bytes 1572872 | tf_op jit(solution)/shard_map/ppermute | solution.py:183
  31.6 22.5 %collective-permute-start.5 = (bf16[64,4096]{1,0:T(8,128)(2,1)S(1)}, bf16[64,4096]{1,0:T(8,128)(2,1)S(1)}, u32[]{:S(2)}, u32[]{:S(2)}) collective-permute-start(bf16[64,4096]{1,0:T(8,128)(2,1)S(1)} %collective-permute-done.refs_2_), channel_id=1, source_target_pairs={{0,2},{1,3},{2,4},{3,5},{4,6},{5,7},{6,0},{7,1},{8,10},{9,11},{10,... | collective-permute-start | bytes 1572872 | tf_op jit(solution)/shard_map/ppermute | solution.py:183
  33.5 21.4 %collective-permute-start.6 = (bf16[64,4096]{1,0:T(8,128)(2,1)S(1)}, bf16[64,4096]{1,0:T(8,128)(2,1)S(1)}, u32[]{:S(2)}, u32[]{:S(2)}) collective-permute-start(bf16[64,4096]{1,0:T(8,128)(2,1)S(1)} %collective-permute-done.1.refs_3_), channel_id=1, source_target_pairs={{0,6},{1,7},{2,0},{3,1},{4,2},{5,3},{6,4},{7,5},{8,14},{9,15},{10,... | collective-permute-start | bytes 1572872 | tf_op jit(solution)/shard_map/ppermute | solution.py:183
  47.7 12.7 %collective-permute-start.7 = (bf16[6,64,256]{2,1,0:T(8,128)(2,1)S(1)}, bf16[6,64,256]{2,1,0:T(8,128)(2,1)S(1)}, u32[]{:S(2)}, u32[]{:S(2)}) collective-permute-start(bf16[6,64,256]{2,1,0:T(8,128)(2,1)S(1)} %get-tuple-element.25), channel_id=1, source_target_pairs={{0,1},{1,0},{2,3},{3,2},{4,5},{5,4},{6,7},{7,6},{8,9},{9,8},{10,11... | collective-permute-start | bytes 589832 | tf_op jit(solution)/shard_map/ppermute | solution.py:183
  56.4 3.9 %collective-permute-start.8 = (bf16[2,64,256]{2,1,0:T(8,128)(2,1)S(1)}, bf16[2,64,256]{2,1,0:T(8,128)(2,1)S(1)}, u32[]{:S(2)}, u32[]{:S(2)}) collective-permute-start(bf16[2,64,256]{2,1,0:T(8,128)(2,1)S(1)} %get-tuple-element.26), channel_id=1, source_target_pairs={{0,1},{1,0},{2,3},{3,2},{4,5},{5,4},{6,7},{7,6},{8,9},{9,8},{10,11... | collective-permute-start | bytes 196616 | tf_op jit(solution)/shard_map/ppermute | solution.py:183
where the time goes:
time: 77.5 us; the launch traced here: 76.6 us
  starting transfers between devices  37.5 us (48%)
  waiting for transfers between devices  14.4 us (19%)
  blocking collectives  13.7 us (18%)
  Pallas kernels  8.17 us (11%)
  local copies, waits for them, and re-layouts  1.94 us (3%)
  between operations  0.9 us (1%)
    ppermute x9, starting transfers between devices, shift(): return lax.ppermute(x, 'tp', by)  37.5 us
    ppermute x9, waiting for transfers between devices, shift(): return lax.ppermute(x, 'tp', by)  14.4 us
    all_to_all x1, blocking collectives, body(): parts = lax.all_to_all(part, 'sp', split_axis=0, concat_axis=0, tiled=True)  13.7 us
    pallas_call x2, Pallas kernels, project(): pl.pallas_call(functools.partial(project_kernel, count), out_shape=(out,...  5.33 us
    unnamed x17, local copies, waits for them, and re-layouts  1.6 us
  transfers between devices with their start and end apart: 9, of which 5 were waited for; matrix products, arithmetic and copies ran while one was open for 0% of the time, Pallas kernels for 7%

commit v1 on v0

--- a/solution.py
+++ b/solution.py
@@ -117,11 +117,12 @@
     half = own1.shape[1]
     members, _, cols = part.shape
     block = keys.shape[1]
-    for side, refs in enumerate(((own1, own2), (got1, got2))):
+    for side, refs in enumerate(((own1, own2), (got1, got2.at[1 - core]))):
         which = lax.rem(core + side, 2)
         for ref, places in zip(refs, (EARLY, LATE)):
             for k, (off, p) in enumerate(places):
-                at = pl.multiple_of((lax.rem(x + off, 4) * 2 + which) * half, half)
+                place = lax.rem(x + jnp.where(which == 0, off, (4 - off) % 4), 4)
+                at = pl.multiple_of((place * 2 + which) * half, half)
                 keys[p, pl.ds(at, half), :] = ref[k, :, :cols]
                 values[p, pl.ds(at, half), :] = ref[k, :, cols:]
     last = lax.axis_index("sp") == lax.axis_size("sp") - 1
@@ -175,6 +176,7 @@
         out_shape=jax.ShapeDtypeStruct((2, cols), jnp.bfloat16),
         in_specs=[VMEM],
         out_specs=VMEM,
+        compiler_params=pltpu.CompilerParams(vmem_limit_bytes=4 * 1024 * 1024),
         name="merge",
     )(parts)
 
@@ -188,17 +190,19 @@
 ):
     members = lax.axis_size("sp")
     tps = lax.axis_size("tp")
-    right = [(i, (i + 2) % tps) for i in range(tps)]
-    left = [(i, (i - 2) % tps) for i in range(tps)]
+    ahead = [(i, (i + 2 - 4 * (i % 2)) % tps) for i in range(tps)]
+    back = [(i, (i - 2 + 4 * (i % 2)) % tps) for i in range(tps)]
     swap = [(i, i ^ 1) for i in range(tps)]
     gain = norm_gain.reshape(1, -1)
-    a0, b0 = tokens[0], tokens[1]
-    a_l = shift(a0, right)
-    b_r = shift(b0, left)
-    b_l = shift(b0, right)
-    a_r = shift(a0, left)
-    a_2 = shift(a_l, right)
-    b_2 = shift(b_r, left)
+    a0 = tokens[0]
+    held, a0 = lax.optimization_barrier((tokens, a0))
+    b0 = held[1]
+    a_3 = shift(a0, ahead)
+    b_1 = shift(b0, back)
+    b_3 = shift(b0, ahead)
+    a_1 = shift(a0, back)
+    a_2 = shift(a_3, ahead)
+    b_2 = shift(b_1, back)
     wo = jnp.concatenate([key_weight, value_weight], axis=1)
     wp = shift(wo, swap)
 
@@ -208,10 +212,11 @@
     gain, wp, made = lax.optimization_barrier((gain, wp, made))
     gates, qm, small = made
 
-    own1, par1 = project((a0, b0, a_l, b_r, a_r, b_l), gain, wo, wp)
+    own1, par1 = project((a0, b0, a_3, b_1, a_1, b_3), gain, wo, wp)
     got1 = shift(par1, swap)
     own2, par2 = project((a_2, b_2), gain, wo, wp)
-    got2 = shift(par2, swap)
+    pairs = [[i, i + 1] for i in range(0, tps, 2)]
+    got2 = lax.all_gather(par2, "tp", axis_index_groups=pairs)
     keys, values, part = attend(own1, own2, got1, got2, gates, qm, small, members)
     parts = lax.all_to_all(part, "sp", split_axis=0, concat_axis=0, tiled=True)
     return keys, values, merge(parts)

time: 77.5 us -> 73.2 us (0.945)
  starting transfers between devices: 37.5 us -> 33.4 us
  blocking collectives: 13.7 us -> 15.5 us
  waiting for transfers between devices: 14.4 us -> 13.4 us
  Pallas kernels: 8.17 us -> 7.28 us
    ppermute x9 -> x8, starting transfers between devices: 37.5 us -> 33.4 us  [shift(): return lax.ppermute(x, 'tp', by)]
    all_gather x0 -> x1, blocking collectives: none -> 2.68 us  [body(): got2 = lax.all_gather(par2, 'tp', axis_index_groups=pairs)]
    ppermute x9 -> x8, waiting for transfers between devices: 14.4 us -> 13.4 us  [shift(): return lax.ppermute(x, 'tp', by)]
    pallas_call x1, Pallas kernels: 1.49 us -> 0.59 us  [merge(): pl.pallas_call(merge_kernel, out_shape=jax.ShapeDtypeStruct((2, cols), jn...]
    all_to_all x1, blocking collectives: 13.7 us -> 12.8 us  [body(): parts = lax.all_to_all(part, 'sp', split_axis=0, concat_axis=0, tiled=True)]
  transfers between devices with their start and end apart: 9 -> 8, of which waited for: 5 -> 5; matrix products, arithmetic and copies ran while one was open for 0% -> 0% of each run, Pallas kernels for 7% -> 8%
where the time goes in v1:
time: 73.2 us; the launch traced here: 72.4 us
  starting transfers between devices  33.4 us (46%)
  blocking collectives  15.5 us (21%)
  waiting for transfers between devices  13.4 us (18%)
  Pallas kernels  7.28 us (10%)
  local copies, waits for them, and re-layouts  1.93 us (3%)
  between operations  0.89 us (1%)
    ppermute x8, starting transfers between devices, shift(): return lax.ppermute(x, 'tp', by)  33.4 us
    ppermute x8, waiting for transfers between devices, shift(): return lax.ppermute(x, 'tp', by)  13.4 us
    all_to_all x1, blocking collectives, body(): parts = lax.all_to_all(part, 'sp', split_axis=0, concat_axis=0, tiled=True)  12.8 us
    pallas_call x2, Pallas kernels, project(): pl.pallas_call(functools.partial(project_kernel, count), out_shape=(out,...  5.33 us
    all_gather x1, blocking collectives, body(): got2 = lax.all_gather(par2, 'tp', axis_index_groups=pairs)  2.68 us
    unnamed x17, local copies, waits for them, and re-layouts  1.6 us
  transfers between devices with their start and end apart: 8, of which 5 were waited for; matrix products, arithmetic and copies ran while one was open for 0% of the time, Pallas kernels for 8%

profile of v1, /device:TPU:1, one launch (start us, length us, event | category | flops | bytes accessed | tf_op | source)
XLA Modules:
  0.0 72.4 jit_solution(686785536180262400)
XLA Ops:
  0.6 0.0 copy-start.5
  0.6 0.0 copy-start.6
  0.7 1.6 %constant_dynamic-update-slice_fusion.1 = bf16[4096,256]{1,0:T(8,128)(2,1)S(1)} fusion(bf16[4096,128]{1,0:T(8,128)(2,1)} %param.11), kind=kLoop, calls=%fused_computation.3 | loop fusion | bytes 2097152
  2.2 0.0 copy-done.5
  2.2 0.0 copy-start.7
  2.2 0.0 copy-start
  2.2 0.0 copy-start.1
  2.3 0.0 copy-start.2
  2.3 0.0 copy-start.3
  2.3 0.0 copy-start.4
  2.3 0.2 constant_dynamic-update-slice_fusion.refs_7_.refs_3_
  2.5 12.4 %collective-permute-start.4 = (bf16[4096,256]{1,0:T(8,128)(2,1)S(1)}, bf16[4096,256]{1,0:T(8,128)(2,1)S(1)}, u32[]{:S(2)}, u32[]{:S(2)}) collective-permute-start(bf16[4096,256]{1,0:T(8,128)(2,1)S(1)} %constant_dynamic-update-slice_fusion.refs_7_.refs_3_), channel_id=1, source_target_pairs={{0,1},{1,0},{2,3},{3,2},{4,5},{5,4},{6,7},{7,6},{8,9},{9,8},{10,11... | collective-permute-start | bytes 6291464 | tf_op jit(solution)/shard_map/ppermute | solution.py:185
  14.9 0.0 copy-done.6
  15.0 1.9 %collective-permute-start.1 = (bf16[64,4096]{1,0:T(8,128)(2,1)S(1)}, bf16[64,4096]{1,0:T(8,128)(2,1)S(1)}, u32[]{:S(2)}, u32[]{:S(2)}) collective-permute-start(bf16[64,4096]{1,0:T(8,128)(2,1)S(1)} %slice_bitcast_fusion.refs_1_), channel_id=1, source_target_pairs={{0,6},{1,3},{2,0},{3,5},{4,2},{5,7},{6,4},{7,1},{8,14},{9,11},{10,... | collective-permute-start | bytes 1572872 | tf_op jit(solution)/shard_map/ppermute | solution.py:185
  17.0 4.6 %collective-permute-start = (bf16[64,4096]{1,0:T(8,128)(2,1)S(1)}, bf16[64,4096]{1,0:T(8,128)(2,1)S(1)}, u32[]{:S(2)}, u32[]{:S(2)}) collective-permute-start(bf16[64,4096]{1,0:T(8,128)(2,1)S(1)} %slice_bitcast_fusion.1.refs_0_), channel_id=1, source_target_pairs={{0,2},{1,7},{2,4},{3,1},{4,6},{5,3},{6,0},{7,5},{8,10},{9,15},{10,... | collective-permute-start | bytes 1572872 | tf_op jit(solution)/shard_map/ppermute | solution.py:185
  21.5 1.9 %collective-permute-start.3 = (bf16[64,4096]{1,0:T(8,128)(2,1)S(1)}, bf16[64,4096]{1,0:T(8,128)(2,1)S(1)}, u32[]{:S(2)}, u32[]{:S(2)}) collective-permute-start(bf16[64,4096]{1,0:T(8,128)(2,1)S(1)} %slice_bitcast_fusion.refs_1_), channel_id=1, source_target_pairs={{0,2},{1,7},{2,4},{3,1},{4,6},{5,3},{6,0},{7,5},{8,10},{9,15},{10,... | collective-permute-start | bytes 1572872 | tf_op jit(solution)/shard_map/ppermute | solution.py:185
  23.5 3.4 %collective-permute-start.2 = (bf16[64,4096]{1,0:T(8,128)(2,1)S(1)}, bf16[64,4096]{1,0:T(8,128)(2,1)S(1)}, u32[]{:S(2)}, u32[]{:S(2)}) collective-permute-start(bf16[64,4096]{1,0:T(8,128)(2,1)S(1)} %slice_bitcast_fusion.1.refs_0_), channel_id=1, source_target_pairs={{0,6},{1,3},{2,0},{3,5},{4,2},{5,7},{6,4},{7,1},{8,14},{9,11},{10,... | collective-permute-start | bytes 1572872 | tf_op jit(solution)/shard_map/ppermute | solution.py:185
  26.8 2.8 %collective-permute-done.1.refs_3_ = bf16[64,4096]{1,0:T(8,128)(2,1)S(1)} collective-permute-done((bf16[64,4096]{1,0:T(8,128)(2,1)S(1)}, bf16[64,4096]{1,0:T(8,128)(2,1)S(1)}, u32[]{:S(2)}, u32[]{:S(2)}) %collective-permute-start.1) | collective-permute-done | bytes 524320 | tf_op jit(solution)/shard_map/ppermute | solution.py:185
  29.7 1.9 %collective-permute-start.6 = (bf16[64,4096]{1,0:T(8,128)(2,1)S(1)}, bf16[64,4096]{1,0:T(8,128)(2,1)S(1)}, u32[]{:S(2)}, u32[]{:S(2)}) collective-permute-start(bf16[64,4096]{1,0:T(8,128)(2,1)S(1)} %collective-permute-done.1.refs_3_), channel_id=1, source_target_pairs={{0,6},{1,3},{2,0},{3,5},{4,2},{5,7},{6,4},{7,1},{8,14},{9,11},{10,... | collective-permute-start | bytes 1572872 | tf_op jit(solution)/shard_map/ppermute | solution.py:185
  31.6 1.2 %collective-permute-done.refs_2_ = bf16[64,4096]{1,0:T(8,128)(2,1)S(1)} collective-permute-done((bf16[64,4096]{1,0:T(8,128)(2,1)S(1)}, bf16[64,4096]{1,0:T(8,128)(2,1)S(1)}, u32[]{:S(2)}, u32[]{:S(2)}) %collective-permute-start) | collective-permute-done | bytes 524320 | tf_op jit(solution)/shard_map/ppermute | solution.py:185
  32.8 3.4 %collective-permute-start.5 = (bf16[64,4096]{1,0:T(8,128)(2,1)S(1)}, bf16[64,4096]{1,0:T(8,128)(2,1)S(1)}, u32[]{:S(2)}, u32[]{:S(2)}) collective-permute-start(bf16[64,4096]{1,0:T(8,128)(2,1)S(1)} %collective-permute-done.refs_2_), channel_id=1, source_target_pairs={{0,2},{1,7},{2,4},{3,1},{4,6},{5,3},{6,0},{7,5},{8,10},{9,15},{10,... | collective-permute-start | bytes 1572872 | tf_op jit(solution)/shard_map/ppermute | solution.py:185
  36.2 0.0 copy-done.7
  36.2 0.0 copy-done
  36.2 0.0 copy-done.1
  36.2 0.0 copy-done.2
  36.2 0.0 copy-done.3
  36.3 0.0 copy-done.4
  36.3 0.3 prepare.1
  36.5 0.0 collective-permute-done.4.refs_8_.refs_4_
  36.5 7.5 %collective-permute-done.3.refs_5_ = bf16[64,4096]{1,0:T(8,128)(2,1)S(1)} collective-permute-done((bf16[64,4096]{1,0:T(8,128)(2,1)S(1)}, bf16[64,4096]{1,0:T(8,128)(2,1)S(1)}, u32[]{:S(2)}, u32[]{:S(2)}) %collective-permute-start.3) | collective-permute-done | bytes 524320 | tf_op jit(solution)/shard_map/ppermute | solution.py:185
  44.0 0.0 collective-permute-done.2.refs_4_
  44.0 3.9 %project.2 = (bf16[6,64,256]{2,1,0:T(8,128)(2,1)S(1)}, bf16[6,64,256]{2,1,0:T(8,128)(2,1)S(1)}) custom-call(bf16[64,4096]{1,0:T(8,128)(2,1)S(1)} %slice_bitcast_fusion.1.refs_0_, bf16[64,4096]{1,0:T(8,128)(2,1)S(1)} %slice_bitcast_fusion.refs_1_, bf16[64,4096]{1,0:T(8,128)(2,1)S(1)} %collective-permute-done.refs_2_, ...), custom_call_target="tpu_custom_call" | custom-call | flops 1610612736 | bytes 6291456 | tf_op jit(solution)/shard_map/project/pallas_call | solution.py:60
  48.0 4.0 %collective-permute-start.7 = (bf16[6,64,256]{2,1,0:T(8,128)(2,1)S(1)}, bf16[6,64,256]{2,1,0:T(8,128)(2,1)S(1)}, u32[]{:S(2)}, u32[]{:S(2)}) collective-permute-start(bf16[6,64,256]{2,1,0:T(8,128)(2,1)S(1)} %get-tuple-element.29), channel_id=1, source_target_pairs={{0,1},{1,0},{2,3},{3,2},{4,5},{5,4},{6,7},{7,6},{8,9},{9,8},{10,11... | collective-permute-start | bytes 589832 | tf_op jit(solution)/shard_map/ppermute | solution.py:185
  52.0 0.2 collective-permute-done.6.refs_1_
  52.2 1.7 %collective-permute-done.5.refs_0_ = bf16[64,4096]{1,0:T(8,128)(2,1)S(1)} collective-permute-done((bf16[64,4096]{1,0:T(8,128)(2,1)S(1)}, bf16[64,4096]{1,0:T(8,128)(2,1)S(1)}, u32[]{:S(2)}, u32[]{:S(2)}) %collective-permute-start.5) | collective-permute-done | bytes 524320 | tf_op jit(solution)/shard_map/ppermute | solution.py:185
  53.8 1.4 %project.3 = (bf16[2,64,256]{2,1,0:T(8,128)(2,1)S(1)}, bf16[2,64,256]{2,1,0:T(8,128)(2,1)S(1)}) custom-call(bf16[64,4096]{1,0:T(8,128)(2,1)S(1)} %collective-permute-done.5.refs_0_, bf16[64,4096]{1,0:T(8,128)(2,1)S(1)} %collective-permute-done.6.refs_1_, bf16[1,4096]{1,0:T(2,128)(2,1)S(1)} %reshape.9.refs_6_.refs_2_, ...), custom_call_target="tpu_custom_call" | custom-call | flops 536870912 | bytes 6291456 | tf_op jit(solution)/shard_map/project/pallas_call | solution.py:60
  55.2 2.7 %all-gather = bf16[4,64,256]{2,1,0:T(8,128)(2,1)S(1)} all-gather(bf16[2,64,256]{2,1,0:T(8,128)(2,1)S(1)} %get-tuple-element.30), channel_id=2, replica_groups={{0,1},{2,3},{4,5},{6,7},{8,9},{10,11},{12,13},{14,15},{16,17},{18,19},{..., dimensions={0}, use_global_device_ids=true | all-gather | bytes 196608 | tf_op jit(solution)/shard_map/all_gather | solution.py:219
  57.9 0.0 collective-permute-done.7.got1
  57.9 1.1 %attend.1 = (bf16[2,512,128]{2,1,0:T(8,128)(2,1)}, bf16[2,512,128]{2,1,0:T(8,128)(2,1)}, f32[32,8,128]{2,1,0:T(8,128)S(1)}) custom-call(bf16[6,64,256]{2,1,0:T(8,128)(2,1)S(1)} %get-tuple-element.27.own1, bf16[2,64,256]{2,1,0:T(8,128)(2,1)S(1)} %get-tuple-element.28.own2, bf16[6,64,256]{2,1,0:T(8,128)(2,1)S(1)} %collective-permute-done.7.got1, ...), custom_call_target="tpu_custom_call" | custom-call | flops 67108864 | bytes 2097152 | tf_op jit(solution)/shard_map/attend/pallas_call | solution.py:149
  59.0 12.8 %all_to_all.5.parts = f32[32,8,128]{2,1,0:T(8,128)S(1)} all-to-all(f32[32,8,128]{2,1,0:T(8,128)S(1)} %get-tuple-element.36), channel_id=1, replica_groups=mesh['gr'=3,'sp'=32,'tp'=8] {'sp'}, dimensions={0} | all-to-all | bytes 262144 | tf_op jit(solution)/shard_map/all_to_all | solution.py:221
  71.8 0.6 merge.1
  (3 shorter events, 0.1 us)
Async XLA Ops:
  0.6 1.6 %copy-start.5 = (bf16[4096,128]{1,0:T(8,128)(2,1)S(1)}, bf16[4096,128]{1,0:T(8,128)(2,1)}, u32[]{:S(2)}) copy-start(bf16[4096,128]{1,0:T(8,128)(2,1)} %param.12) | copy-start | bytes 3145732
  0.6 14.3 %copy-start.6 = (bf16[2,64,4096]{2,1,0:T(8,128)(2,1)S(1)}, bf16[2,64,4096]{2,1,0:T(8,128)(2,1)}, u32[]{:S(2)}) copy-start(bf16[2,64,4096]{2,1,0:T(8,128)(2,1)} %param.9) | copy-start | bytes 3145732
  2.2 34.0 %copy-start.7 = (bf16[4096]{0:T(1024)(128)(2,1)S(1)}, bf16[4096]{0:T(1024)(128)(2,1)}, u32[]{:S(2)}) copy-start(bf16[4096]{0:T(1024)(128)(2,1)} %param.10) | copy-start | bytes 24580
  2.2 34.0 %copy-start = (f32[2,512,2]{1,2,0:T(2,128)S(1)}, f32[2,512,2]{1,2,0:T(2,128)}, u32[]{:S(2)}) copy-start(f32[2,512,2]{1,2,0:T(2,128)} %param.13) | copy-start | bytes 24580
  2.2 34.0 %copy-start.1 = (f32[2,2]{1,0:T(2,128)S(1)}, f32[2,2]{1,0:T(2,128)}, u32[]{:S(2)}) copy-start(f32[2,2]{1,0:T(2,128)} %ng.1) | copy-start | bytes 52
  2.3 34.0 %copy-start.2 = (bf16[2,128]{1,0:T(2,128)(2,1)S(1)}, bf16[2,128]{1,0:T(2,128)(2,1)}, u32[]{:S(2)}) copy-start(bf16[2,128]{1,0:T(2,128)(2,1)} %q.1) | copy-start | bytes 1540
  2.3 34.0 %copy-start.3 = (bf16[2,128]{1,0:T(2,128)(2,1)S(1)}, bf16[2,128]{1,0:T(2,128)(2,1)}, u32[]{:S(2)}) copy-start(bf16[2,128]{1,0:T(2,128)(2,1)} %fk.1) | copy-start | bytes 1540
  2.3 34.0 %copy-start.4 = (bf16[2,128]{1,0:T(2,128)(2,1)S(1)}, bf16[2,128]{1,0:T(2,128)(2,1)}, u32[]{:S(2)}) copy-start(bf16[2,128]{1,0:T(2,128)(2,1)} %fv.1) | copy-start | bytes 1540
  2.5 34.0 %collective-permute-start.4 = (bf16[4096,256]{1,0:T(8,128)(2,1)S(1)}, bf16[4096,256]{1,0:T(8,128)(2,1)S(1)}, u32[]{:S(2)}, u32[]{:S(2)}) collective-permute-start(bf16[4096,256]{1,0:T(8,128)(2,1)S(1)} %constant_dynamic-update-slice_fusion.refs_7_.refs_3_), channel_id=1, source_target_pairs={{0,1},{1,0},{2,3},{3,2},{4,5},{5,4},{6,7},{7,6},{8,9},{9,8},{10,11... | collective-permute-start | bytes 6291464 | tf_op jit(solution)/shard_map/ppermute | solution.py:185
  15.0 14.6 %collective-permute-start.1 = (bf16[64,4096]{1,0:T(8,128)(2,1)S(1)}, bf16[64,4096]{1,0:T(8,128)(2,1)S(1)}, u32[]{:S(2)}, u32[]{:S(2)}) collective-permute-start(bf16[64,4096]{1,0:T(8,128)(2,1)S(1)} %slice_bitcast_fusion.refs_1_), channel_id=1, source_target_pairs={{0,6},{1,3},{2,0},{3,5},{4,2},{5,7},{6,4},{7,1},{8,14},{9,11},{10,... | collective-permute-start | bytes 1572872 | tf_op jit(solution)/shard_map/ppermute | solution.py:185
  17.0 15.8 %collective-permute-start = (bf16[64,4096]{1,0:T(8,128)(2,1)S(1)}, bf16[64,4096]{1,0:T(8,128)(2,1)S(1)}, u32[]{:S(2)}, u32[]{:S(2)}) collective-permute-start(bf16[64,4096]{1,0:T(8,128)(2,1)S(1)} %slice_bitcast_fusion.1.refs_0_), channel_id=1, source_target_pairs={{0,2},{1,7},{2,4},{3,1},{4,6},{5,3},{6,0},{7,5},{8,10},{9,15},{10,... | collective-permute-start | bytes 1572872 | tf_op jit(solution)/shard_map/ppermute | solution.py:185
  21.5 22.5 %collective-permute-start.3 = (bf16[64,4096]{1,0:T(8,128)(2,1)S(1)}, bf16[64,4096]{1,0:T(8,128)(2,1)S(1)}, u32[]{:S(2)}, u32[]{:S(2)}) collective-permute-start(bf16[64,4096]{1,0:T(8,128)(2,1)S(1)} %slice_bitcast_fusion.refs_1_), channel_id=1, source_target_pairs={{0,2},{1,7},{2,4},{3,1},{4,6},{5,3},{6,0},{7,5},{8,10},{9,15},{10,... | collective-permute-start | bytes 1572872 | tf_op jit(solution)/shard_map/ppermute | solution.py:185
  23.5 20.6 %collective-permute-start.2 = (bf16[64,4096]{1,0:T(8,128)(2,1)S(1)}, bf16[64,4096]{1,0:T(8,128)(2,1)S(1)}, u32[]{:S(2)}, u32[]{:S(2)}) collective-permute-start(bf16[64,4096]{1,0:T(8,128)(2,1)S(1)} %slice_bitcast_fusion.1.refs_0_), channel_id=1, source_target_pairs={{0,6},{1,3},{2,0},{3,5},{4,2},{5,7},{6,4},{7,1},{8,14},{9,11},{10,... | collective-permute-start | bytes 1572872 | tf_op jit(solution)/shard_map/ppermute | solution.py:185
  29.7 22.5 %collective-permute-start.6 = (bf16[64,4096]{1,0:T(8,128)(2,1)S(1)}, bf16[64,4096]{1,0:T(8,128)(2,1)S(1)}, u32[]{:S(2)}, u32[]{:S(2)}) collective-permute-start(bf16[64,4096]{1,0:T(8,128)(2,1)S(1)} %collective-permute-done.1.refs_3_), channel_id=1, source_target_pairs={{0,6},{1,3},{2,0},{3,5},{4,2},{5,7},{6,4},{7,1},{8,14},{9,11},{10,... | collective-permute-start | bytes 1572872 | tf_op jit(solution)/shard_map/ppermute | solution.py:185
  32.8 21.0 %collective-permute-start.5 = (bf16[64,4096]{1,0:T(8,128)(2,1)S(1)}, bf16[64,4096]{1,0:T(8,128)(2,1)S(1)}, u32[]{:S(2)}, u32[]{:S(2)}) collective-permute-start(bf16[64,4096]{1,0:T(8,128)(2,1)S(1)} %collective-permute-done.refs_2_), channel_id=1, source_target_pairs={{0,2},{1,7},{2,4},{3,1},{4,6},{5,3},{6,0},{7,5},{8,10},{9,15},{10,... | collective-permute-start | bytes 1572872 | tf_op jit(solution)/shard_map/ppermute | solution.py:185
  48.0 10.0 %collective-permute-start.7 = (bf16[6,64,256]{2,1,0:T(8,128)(2,1)S(1)}, bf16[6,64,256]{2,1,0:T(8,128)(2,1)S(1)}, u32[]{:S(2)}, u32[]{:S(2)}) collective-permute-start(bf16[6,64,256]{2,1,0:T(8,128)(2,1)S(1)} %get-tuple-element.29), channel_id=1, source_target_pairs={{0,1},{1,0},{2,3},{3,2},{4,5},{5,4},{6,7},{7,6},{8,9},{9,8},{10,11... | collective-permute-start | bytes 589832 | tf_op jit(solution)/shard_map/ppermute | solution.py:185

commit v2 on v1

--- a/solution.py
+++ b/solution.py
@@ -14,14 +14,17 @@
 
 
 VMEM = pl.BlockSpec(memory_space=pltpu.VMEM)
-
-EARLY = ((0, 0), (0, 1), (3, 0), (1, 1), (1, 0), (3, 1))
+ANY = pl.BlockSpec(memory_space=pl.ANY)
+
+EARLY = ((0, 0), (0, 1), (3, 0), (3, 1), (1, 0), (1, 1))
 LATE = ((2, 0), (2, 1))
 
 
-def project_kernel(count, *refs):
-    xs, (gain, wo, wp, own, par, n_s) = refs[:count], refs[count:]
-    half, width = xs[0].shape
+def project_kernel(count, prior, *refs):
+    xs, refs = refs[:count], refs[count:]
+    before, (gain, wo, wp, own, par, n_s) = refs[: 2 * prior], refs[2 * prior :]
+    width = xs[0].shape[1]
+    half = own.shape[1]
     step = 16
 
     def normalize(x, base):
@@ -43,34 +46,39 @@
                 n_s[out, at] = part.astype(jnp.bfloat16)
             return carry
 
-        lax.fori_loop(0, half // step, rows_of, 0, unroll=2)
-
-    for k, x in enumerate(xs):
-        normalize(x, k * half)
-    for w, out in ((wo, own), (wp, par)):
+        lax.fori_loop(0, x.shape[0] // step, rows_of, 0, unroll=2)
+
+    base = 0
+    for x in xs:
+        normalize(x, base)
+        base += x.shape[0]
+    for k, (w, out) in enumerate(((wo, own), (wp, par))):
         acc = jnp.dot(n_s[...], w[...], preferred_element_type=jnp.float32)
-        out[...] = acc.astype(jnp.bfloat16).reshape(out.shape)
-
-
-def project(xs, gain, wo, wp):
-    count = len(xs)
-    half, width = xs[0].shape
-    cols = wo.shape[1]
-    out = jax.ShapeDtypeStruct((count, half, cols), jnp.bfloat16)
-    return pl.pallas_call(
-        functools.partial(project_kernel, count),
+        done = before[k].shape[0] if prior else 0
+        if prior:
+            out[:done] = before[k][...]
+        out[done:] = acc.astype(jnp.bfloat16).reshape(-1, half, out.shape[2])
+
+
+def project(xs, gain, wo, wp, half, before=()):
+    rows = sum(x.shape[0] for x in xs)
+    width, cols = wo.shape
+    done = before[0].shape[0] if before else 0
+    out = jax.ShapeDtypeStruct((done + rows // half, half, cols), jnp.bfloat16)
+    return pl.pallas_call(
+        functools.partial(project_kernel, len(xs), bool(before)),
         out_shape=(out, out),
-        in_specs=[VMEM] * (count + 3),
+        in_specs=[VMEM] * (len(xs) + len(before) + 3),
         out_specs=(VMEM, VMEM),
-        scratch_shapes=[pltpu.VMEM((count * half, width), jnp.bfloat16)],
-        compiler_params=pltpu.CompilerParams(vmem_limit_bytes=24 * 1024 * 1024),
+        scratch_shapes=[pltpu.VMEM((rows, width), jnp.bfloat16)],
+        compiler_params=pltpu.CompilerParams(vmem_limit_bytes=16 * 1024 * 1024),
         cost_estimate=pl.CostEstimate(
-            flops=2 * count * half * width * 2 * cols,
+            flops=2 * rows * width * 2 * cols,
             bytes_accessed=6 * 1024 * 1024,
             transcendentals=0,
         ),
         name="project",
-    )(*xs, gain, wo, wp)
+    )(*xs, *before, gain, wo, wp)
 
 
 def prepare_kernel(cum, q, fk, fv, ng, gates, qm, small):
@@ -111,52 +119,124 @@
     )(cum, q, fk, fv, ng)
 
 
-def attend_kernel(own1, own2, got1, got2, gates, qm, small, keys, values, part):
+def halves(own, got, places):
     tp = lax.axis_index("tp")
     x, core = tp // 2, lax.rem(tp, 2)
-    half = own1.shape[1]
+    half = own.shape[1]
+    found = []
+    for side, ref in enumerate((own, got)):
+        which = lax.rem(core + side, 2)
+        for k, (off, p) in enumerate(places):
+            place = lax.rem(x + jnp.where(which == 0, off, (4 - off) % 4), 4)
+            found.append((ref, k, p, pl.multiple_of((place * 2 + which) * half, half)))
+    return found
+
+
+def stored(found, keys, values, sem):
+    cols = keys.shape[2]
+    copies = []
+    for i, (ref, k, p, at) in enumerate(found):
+        rows = pl.ds(at, ref.shape[1])
+        for j, cache in enumerate((keys, values)):
+            copies.append(
+                pltpu.make_async_copy(
+                    ref.at[k, :, pl.ds(j * cols, cols)], cache.at[p, rows, :], sem.at[i, j]
+                )
+            )
+    for copy in copies:
+        copy.start()
+    return copies
+
+
+def scored(found, p, gates, qm):
+    cols = qm.shape[2]
+    parts, seen = [], []
+    for ref, k, prompt, at in found:
+        if prompt == p:
+            part = jnp.dot(ref[k, :, :cols], qm[p], preferred_element_type=jnp.float32)
+            parts.append(part * (HD**-0.5) - gates[p, pl.ds(at, ref.shape[1]), :])
+            seen.append(ref[k, :, cols:].astype(jnp.float32))
+    return jnp.concatenate(parts, axis=0), jnp.concatenate(seen, axis=0)
+
+
+def early_kernel(own, got, gates, qm, keys, values, state, sem):
+    found = halves(own, got, EARLY)
+    copies = stored(found, keys, values, sem)
+    for p in range(2):
+        scores, seen = scored(found, p, gates, qm)
+        top = jnp.max(scores, axis=0, keepdims=True)
+        weights = jnp.exp(scores - top)
+        state[4 * p : 4 * p + 1, :] = top
+        state[4 * p + 1 : 4 * p + 2, :] = jnp.sum(weights, axis=0, keepdims=True)
+        state[4 * p + 2 : 4 * p + 3, :] = jnp.sum(weights * seen, axis=0, keepdims=True)
+        state[4 * p + 3 : 4 * p + 4, :] = jnp.zeros_like(top)
+    for copy in copies:
+        copy.wait()
+
+
+def early(own, got, gates, qm):
+    block, cols = gates.shape[1:]
+    cache = jax.ShapeDtypeStruct((2, block, cols), jnp.bfloat16)
+    return pl.pallas_call(
+        early_kernel,
+        out_shape=(cache, cache, jax.ShapeDtypeStruct((8, cols), jnp.float32)),
+        in_specs=[VMEM] * 4,
+        out_specs=(ANY, ANY, VMEM),
+        scratch_shapes=[pltpu.SemaphoreType.DMA((2 * len(EARLY), 2))],
+        compiler_params=pltpu.CompilerParams(vmem_limit_bytes=8 * 1024 * 1024),
+        cost_estimate=pl.CostEstimate(
+            flops=64 * 1024 * 1024, bytes_accessed=2 * 1024 * 1024, transcendentals=0
+        ),
+        name="early",
+    )(own, got, gates, qm)
+
+
+def late_kernel(own, both, gates, qm, small, state, k_in, v_in, keys, values, part, sem):
+    core = lax.rem(lax.axis_index("tp"), 2)
+    found = halves(own, both.at[1 - core], LATE)
+    copies = stored(found, keys, values, sem)
     members, _, cols = part.shape
-    block = keys.shape[1]
-    for side, refs in enumerate(((own1, own2), (got1, got2.at[1 - core]))):
-        which = lax.rem(core + side, 2)
-        for ref, places in zip(refs, (EARLY, LATE)):
-            for k, (off, p) in enumerate(places):
-                place = lax.rem(x + jnp.where(which == 0, off, (4 - off) % 4), 4)
-                at = pl.multiple_of((place * 2 + which) * half, half)
-                keys[p, pl.ds(at, half), :] = ref[k, :, :cols]
-                values[p, pl.ds(at, half), :] = ref[k, :, cols:]
+    block = gates.shape[1]
     last = lax.axis_index("sp") == lax.axis_size("sp") - 1
-    s0, fv, fg = small[0:2, :], small[2:4, :], small[4:6, :]
     for p in range(2):
-        one = slice(p, p + 1)
-        scores = jnp.dot(keys[p], qm[p], preferred_element_type=jnp.float32)
-        scores = scores * (HD**-0.5) - gates[p]
-        fresh = s0[one] - (gates[p, block - 1 : block, :] + fg[one])
+        scores, seen = scored(found, p, gates, qm)
+        fresh = small[p : p + 1, :] - (
+            gates[p, block - 1 : block, :] + small[4 + p : 5 + p, :]
+        )
         fresh = jnp.where(last, fresh, MASKED)
+        before = state[4 * p : 4 * p + 1, :]
         top = jnp.maximum(jnp.max(scores, axis=0, keepdims=True), fresh)
+        top = jnp.maximum(top, before)
         weights = jnp.exp(scores - top)
         fresh_weight = jnp.exp(fresh - top)
+        scale = jnp.exp(before - top)
         total = jnp.sum(weights, axis=0, keepdims=True) + fresh_weight
-        acc = jnp.sum(weights * values[p].astype(jnp.float32), axis=0, keepdims=True)
-        acc = acc + fresh_weight * fv[one]
+        total = total + scale * state[4 * p + 1 : 4 * p + 2, :]
+        acc = jnp.sum(weights * seen, axis=0, keepdims=True)
+        acc = acc + fresh_weight * small[2 + p : 3 + p, :]
+        acc = acc + scale * state[4 * p + 2 : 4 * p + 3, :]
         for r, row in ((2 * p, top), (2 * p + 1, top), (2 * p + 4, total), (2 * p + 5, acc)):
             part[:, r : r + 1, :] = jnp.broadcast_to(row[None], (members, 1, cols))
-
-
-def attend(own1, own2, got1, got2, gates, qm, small, members):
-    block, cols = gates.shape[1:]
-    cache = jax.ShapeDtypeStruct((2, block, cols), jnp.bfloat16)
-    return pl.pallas_call(
-        attend_kernel,
+    for copy in copies:
+        copy.wait()
+
+
+def late(own, both, gates, qm, small, state, keys, values, members):
+    cols = gates.shape[2]
+    cache = jax.ShapeDtypeStruct(keys.shape, keys.dtype)
+    return pl.pallas_call(
+        late_kernel,
         out_shape=(cache, cache, jax.ShapeDtypeStruct((members, 8, cols), jnp.float32)),
-        in_specs=[VMEM] * 7,
-        out_specs=(VMEM, VMEM, VMEM),
-        compiler_params=pltpu.CompilerParams(vmem_limit_bytes=16 * 1024 * 1024),
+        in_specs=[VMEM] * 6 + [ANY, ANY],
+        out_specs=(ANY, ANY, VMEM),
+        input_output_aliases={6: 0, 7: 1},
+        scratch_shapes=[pltpu.SemaphoreType.DMA((2 * len(LATE), 2))],
+        compiler_params=pltpu.CompilerParams(vmem_limit_bytes=8 * 1024 * 1024),
         cost_estimate=pl.CostEstimate(
-            flops=64 * 1024 * 1024, bytes_accessed=2 * 1024 * 1024, transcendentals=0
-        ),
-        name="attend",
-    )(own1, own2, got1, got2, gates, qm, small)
+            flops=16 * 1024 * 1024, bytes_accessed=1024 * 1024, transcendentals=0
+        ),
+        name="late",
+    )(own, both, gates, qm, small, state, keys, values)
 
 
 def merge_kernel(parts, out):
@@ -194,15 +274,11 @@
     back = [(i, (i - 2 + 4 * (i % 2)) % tps) for i in range(tps)]
     swap = [(i, i ^ 1) for i in range(tps)]
     gain = norm_gain.reshape(1, -1)
-    a0 = tokens[0]
-    held, a0 = lax.optimization_barrier((tokens, a0))
-    b0 = held[1]
-    a_3 = shift(a0, ahead)
-    b_1 = shift(b0, back)
-    b_3 = shift(b0, ahead)
-    a_1 = shift(a0, back)
-    a_2 = shift(a_3, ahead)
-    b_2 = shift(b_1, back)
+    half, width = tokens.shape[1:]
+    from_3 = shift(tokens, ahead)
+    from_1 = shift(tokens, back)
+    a_2 = shift(from_3[0], ahead)
+    b_2 = shift(from_1[1], back)
     wo = jnp.concatenate([key_weight, value_weight], axis=1)
     wp = shift(wo, swap)
 
@@ -212,12 +288,18 @@
     gain, wp, made = lax.optimization_barrier((gain, wp, made))
     gates, qm, small = made
 
-    own1, par1 = project((a0, b0, a_3, b_1, a_1, b_3), gain, wo, wp)
+    rows = (2 * half, width)
+    done = project((tokens.reshape(rows),), gain, wo, wp, half)
+    own1, par1 = project((from_3.reshape(rows), from_1.reshape(rows)), gain, wo, wp, half, done)
     got1 = shift(par1, swap)
-    own2, par2 = project((a_2, b_2), gain, wo, wp)
+    done = project((a_2,), gain, wo, wp, half)
+    keys, values, state = early(own1, got1, gates, qm)
+    own2, par2 = project((b_2,), gain, wo, wp, half, done)
     pairs = [[i, i + 1] for i in range(0, tps, 2)]
-    got2 = lax.all_gather(par2, "tp", axis_index_groups=pairs)
-    keys, values, part = attend(own1, own2, got1, got2, gates, qm, small, members)
+    both2 = lax.all_gather(par2, "tp", axis_index_groups=pairs)
+    keys, values, part = late(
+        own2, both2, gates, qm, small, state, keys, values, members
+    )
     parts = lax.all_to_all(part, "sp", split_axis=0, concat_axis=0, tiled=True)
     return keys, values, merge(parts)
 

time: 73.2 us -> 75 us (1.025)
  the two profiles are of different devices: /device:TPU:1 before, /device:TPU:4 now
where the time goes in v2:
time: 75 us; the launch traced here: 74.7 us
  blocking collectives  24.6 us (33%)
  waiting for transfers between devices  20.6 us (27%)
  starting transfers between devices  17.4 us (23%)
  Pallas kernels  9.37 us (12%)
  local copies, waits for them, and re-layouts  1.79 us (2%)
  between operations  0.9 us (1%)
    all_to_all x1, blocking collectives, body(): parts = lax.all_to_all(part, 'sp', split_axis=0, concat_axis=0, tiled=True)  22.7 us
    ppermute x6, waiting for transfers between devices, shift(): return lax.ppermute(x, 'tp', by)  20.6 us
    ppermute x6, starting transfers between devices, shift(): return lax.ppermute(x, 'tp', by)  17.4 us
    pallas_call x4, Pallas kernels, project(): pl.pallas_call(functools.partial(project_kernel, len(xs), bool(before)),...  6.45 us
    all_gather x1, blocking collectives, body(): both2 = lax.all_gather(par2, 'tp', axis_index_groups=pairs)  1.9 us
  transfers between devices with their start and end apart: 6, of which 3 were waited for; matrix products, arithmetic and copies ran while one was open for 2% of the time, Pallas kernels for 9%

profile of v2, /device:TPU:4, one launch (start us, length us, event | category | flops | bytes accessed | tf_op | source)
XLA Modules:
  0.0 74.7 jit_solution(143984854251398284)
XLA Ops:
  0.6 0.0 copy-start.6
  0.6 3.2 %collective-permute-start.2 = (bf16[2,64,4096]{2,1,0:T(8,128)(2,1)}, bf16[2,64,4096]{2,1,0:T(8,128)(2,1)S(1)}, u32[]{:S(2)}, u32[]{:S(2)}) collective-permute-start(bf16[2,64,4096]{2,1,0:T(8,128)(2,1)} %param.9), channel_id=1, source_target_pairs={{0,2},{1,7},{2,4},{3,1},{4,6},{5,3},{6,0},{7,5},{8,10},{9,15},{10,... | collective-permute-start | bytes 3145736 | tf_op jit(solution)/shard_map/ppermute | solution.py:265
  3.9 2.7 %collective-permute-start = (bf16[2,64,4096]{2,1,0:T(8,128)(2,1)}, bf16[2,64,4096]{2,1,0:T(8,128)(2,1)S(1)}, u32[]{:S(2)}, u32[]{:S(2)}) collective-permute-start(bf16[2,64,4096]{2,1,0:T(8,128)(2,1)} %param.9), channel_id=1, source_target_pairs={{0,6},{1,3},{2,0},{3,5},{4,2},{5,7},{6,4},{7,1},{8,14},{9,11},{10,... | collective-permute-start | bytes 3145736 | tf_op jit(solution)/shard_map/ppermute | solution.py:265
  6.6 1.4 %constant_dynamic-update-slice_fusion.1 = bf16[4096,256]{1,0:T(8,128)(2,1)S(1)} fusion(bf16[4096,128]{1,0:T(8,128)(2,1)} %param.11), kind=kLoop, calls=%fused_computation.3 | loop fusion | bytes 2097152
  8.0 0.0 copy-done.6
  8.1 0.0 copy-start.7
  8.1 0.0 copy-start.1
  8.1 0.0 copy-start.2
  8.1 0.0 copy-start.3
  8.1 0.0 copy-start.4
  8.1 0.0 copy-start.5
  8.1 0.0 copy-start
  8.1 0.2 constant_dynamic-update-slice_fusion.refs_2_.refs_4_.refs_5_
  8.4 2.1 %collective-permute-start.4 = (bf16[4096,256]{1,0:T(8,128)(2,1)S(1)}, bf16[4096,256]{1,0:T(8,128)(2,1)S(1)}, u32[]{:S(2)}, u32[]{:S(2)}) collective-permute-start(bf16[4096,256]{1,0:T(8,128)(2,1)S(1)} %constant_dynamic-update-slice_fusion.refs_2_.refs_4_.refs_5_), channel_id=1, source_target_pairs={{0,1},{1,0},{2,3},{3,2},{4,5},{5,4},{6,7},{7,6},{8,9},{9,8},{10,11... | collective-permute-start | bytes 6291464 | tf_op jit(solution)/shard_map/ppermute | solution.py:265
  10.5 17.4 %collective-permute-done.2 = bf16[2,64,4096]{2,1,0:T(8,128)(2,1)S(1)} collective-permute-done((bf16[2,64,4096]{2,1,0:T(8,128)(2,1)}, bf16[2,64,4096]{2,1,0:T(8,128)(2,1)S(1)}, u32[]{:S(2)}, u32[]{:S(2)}) %collective-permute-start.2) | collective-permute-done | bytes 1048608 | tf_op jit(solution)/shard_map/ppermute | solution.py:265
  27.9 5.5 %collective-permute-start.3 = (bf16[64,4096]{1,0:T(8,128)(2,1)S(1)}, bf16[64,4096]{1,0:T(8,128)(2,1)S(1)}, u32[]{:S(2)}, u32[]{:S(2)}) collective-permute-start(bf16[64,4096]{1,0:T(8,128)(2,1)S(1)} %slice_bitcast_fusion), channel_id=1, source_target_pairs={{0,2},{1,7},{2,4},{3,1},{4,6},{5,3},{6,0},{7,5},{8,10},{9,15},{10,... | collective-permute-start | bytes 1572872 | tf_op jit(solution)/shard_map/ppermute | solution.py:265
  33.4 0.0 collective-permute-done
  33.5 2.0 %collective-permute-start.1 = (bf16[64,4096]{1,0:T(8,128)(2,1)S(1)}, bf16[64,4096]{1,0:T(8,128)(2,1)S(1)}, u32[]{:S(2)}, u32[]{:S(2)}) collective-permute-start(bf16[64,4096]{1,0:T(8,128)(2,1)S(1)} %slice_bitcast_fusion.1), channel_id=1, source_target_pairs={{0,6},{1,3},{2,0},{3,5},{4,2},{5,7},{6,4},{7,1},{8,14},{9,11},{10,... | collective-permute-start | bytes 1572872 | tf_op jit(solution)/shard_map/ppermute | solution.py:265
  35.4 0.0 copy-done.7
  35.5 0.0 copy-done.1
  35.5 0.0 copy-done.2
  35.5 0.0 copy-done.3
  35.5 0.0 copy-done.4
  35.5 0.0 copy-done.5
  35.5 0.3 prepare.1
  35.8 0.0 collective-permute-done.4.refs_3_.refs_5_.refs_6_
  35.8 0.0 copy-done
  35.8 1.4 %project.6 = (bf16[2,64,256]{2,1,0:T(8,128)(2,1)S(1)}, bf16[2,64,256]{2,1,0:T(8,128)(2,1)S(1)}) custom-call(bf16[128,4096]{1,0:T(8,128)(2,1)S(1)} %bitcast.11, bf16[1,4096]{1,0:T(2,128)(2,1)S(1)} %reshape.18.refs_1_.refs_3_.refs_4_, bf16[4096,256]{1,0:T(8,128)(2,1)S(1)} %constant_dynamic-update-slice_fusion.refs_2_.refs_4_.refs_5_, ...), custom_call_target="tpu_custom_call" | custom-call | flops 536870912 | bytes 6291456 | tf_op jit(solution)/shard_map/project/pallas_call | solution.py:68
  37.2 2.7 %project.7 = (bf16[6,64,256]{2,1,0:T(8,128)(2,1)S(1)}, bf16[6,64,256]{2,1,0:T(8,128)(2,1)S(1)}) custom-call(bf16[128,4096]{1,0:T(8,128)(2,1)S(1)} %bitcast.9, bf16[128,4096]{1,0:T(8,128)(2,1)S(1)} %bitcast.10, bf16[2,64,256]{2,1,0:T(8,128)(2,1)S(1)} %get-tuple-element.37.refs_2_, bf16[2,64,256]{2,1,0:T(8,128)(2,1)S(1)} %get-tuple-element.38.refs_3_, ...), custom_call_target="tpu_custom_call" | custom-call | flops 1073741824 | bytes 6291456 | tf_op jit(solution)/shard_map/project/pallas_call | solution.py:68
  39.9 1.9 %collective-permute-start.5 = (bf16[6,64,256]{2,1,0:T(8,128)(2,1)S(1)}, bf16[6,64,256]{2,1,0:T(8,128)(2,1)S(1)}, u32[]{:S(2)}, u32[]{:S(2)}) collective-permute-start(bf16[6,64,256]{2,1,0:T(8,128)(2,1)S(1)} %get-tuple-element.40), channel_id=1, source_target_pairs={{0,1},{1,0},{2,3},{3,2},{4,5},{5,4},{6,7},{7,6},{8,9},{9,8},{10,11... | collective-permute-start | bytes 589832 | tf_op jit(solution)/shard_map/ppermute | solution.py:265
  41.8 2.9 %collective-permute-done.3.refs_0_ = bf16[64,4096]{1,0:T(8,128)(2,1)S(1)} collective-permute-done((bf16[64,4096]{1,0:T(8,128)(2,1)S(1)}, bf16[64,4096]{1,0:T(8,128)(2,1)S(1)}, u32[]{:S(2)}, u32[]{:S(2)}) %collective-permute-start.3) | collective-permute-done | bytes 524320 | tf_op jit(solution)/shard_map/ppermute | solution.py:265
  44.8 1.2 %project.4 = (bf16[1,64,256]{2,1,0:T(8,128)(2,1)S(1)}, bf16[1,64,256]{2,1,0:T(8,128)(2,1)S(1)}) custom-call(bf16[64,4096]{1,0:T(8,128)(2,1)S(1)} %collective-permute-done.3.refs_0_, bf16[1,4096]{1,0:T(2,128)(2,1)S(1)} %reshape.18.refs_1_.refs_3_.refs_4_, bf16[4096,256]{1,0:T(8,128)(2,1)S(1)} %constant_dynamic-update-slice_fusion.refs_2_.refs_4_.refs_5_, ...), custom_call_target="tpu_custom_call" | custom-call | flops 268435456 | bytes 6291456 | tf_op jit(solution)/shard_map/project/pallas_call | solution.py:68
  46.0 0.2 collective-permute-done.1.refs_0_
  46.2 1.2 %project.5 = (bf16[2,64,256]{2,1,0:T(8,128)(2,1)S(1)}, bf16[2,64,256]{2,1,0:T(8,128)(2,1)S(1)}) custom-call(bf16[64,4096]{1,0:T(8,128)(2,1)S(1)} %collective-permute-done.1.refs_0_, bf16[1,64,256]{2,1,0:T(8,128)(2,1)S(1)} %get-tuple-element.30.refs_1_, bf16[1,64,256]{2,1,0:T(8,128)(2,1)S(1)} %get-tuple-element.31.refs_2_, ...), custom_call_target="tpu_custom_call" | custom-call | flops 268435456 | bytes 6291456 | tf_op jit(solution)/shard_map/project/pallas_call | solution.py:68
  47.4 1.9 %all-gather = bf16[4,64,256]{2,1,0:T(8,128)(2,1)S(1)} all-gather(bf16[2,64,256]{2,1,0:T(8,128)(2,1)S(1)} %get-tuple-element.33), channel_id=2, replica_groups={{0,1},{2,3},{4,5},{6,7},{8,9},{10,11},{12,13},{14,15},{16,17},{18,19},{..., dimensions={0}, use_global_device_ids=true | all-gather | bytes 196608 | tf_op jit(solution)/shard_map/all_gather | solution.py:299
  49.3 0.0 collective-permute-done.5.got
  49.3 1.2 %early.1 = (bf16[2,512,128]{2,1,0:T(8,128)(2,1)}, bf16[2,512,128]{2,1,0:T(8,128)(2,1)}, f32[8,128]{1,0:T(8,128)S(1)}) custom-call(bf16[6,64,256]{2,1,0:T(8,128)(2,1)S(1)} %get-tuple-element.39.own, bf16[6,64,256]{2,1,0:T(8,128)(2,1)S(1)} %collective-permute-done.5.got, f32[2,512,128]{2,1,0:T(8,128)S(1)} %get-tuple-element.34.gates, ...), custom_call_target="tpu_custom_call" | custom-call | flops 67108864 | bytes 2097152 | tf_op jit(solution)/shard_map/early/pallas_call | solution.py:180
  50.5 0.9 %late.1 = (bf16[2,512,128]{2,1,0:T(8,128)(2,1)}, bf16[2,512,128]{2,1,0:T(8,128)(2,1)}, f32[32,8,128]{2,1,0:T(8,128)S(1)}) custom-call(bf16[2,64,256]{2,1,0:T(8,128)(2,1)S(1)} %get-tuple-element.32.own, bf16[2,2,64,256]{3,2,1,0:T(8,128)(2,1)S(1)} %bitcast.12, ...), custom_call_target="tpu_custom_call", output_to_operand_aliasing={{0}: (6, {}), {1}: (7, {})} | custom-call | flops 16777216 | bytes 1048576 | tf_op jit(solution)/shard_map/late/pallas_call | solution.py:227
  51.4 22.7 %all_to_all.5.parts = f32[32,8,128]{2,1,0:T(8,128)S(1)} all-to-all(f32[32,8,128]{2,1,0:T(8,128)S(1)} %get-tuple-element.46), channel_id=1, replica_groups=mesh['gr'=3,'sp'=32,'tp'=8] {'sp'}, dimensions={0} | all-to-all | bytes 262144 | tf_op jit(solution)/shard_map/all_to_all | solution.py:303
  74.1 0.6 merge.1
  (3 shorter events, 0.1 us)
Async XLA Ops:
  0.6 7.4 %copy-start.6 = (bf16[4096,128]{1,0:T(8,128)(2,1)S(1)}, bf16[4096,128]{1,0:T(8,128)(2,1)}, u32[]{:S(2)}) copy-start(bf16[4096,128]{1,0:T(8,128)(2,1)} %param.12) | copy-start | bytes 3145732
  0.6 27.2 %collective-permute-start.2 = (bf16[2,64,4096]{2,1,0:T(8,128)(2,1)}, bf16[2,64,4096]{2,1,0:T(8,128)(2,1)S(1)}, u32[]{:S(2)}, u32[]{:S(2)}) collective-permute-start(bf16[2,64,4096]{2,1,0:T(8,128)(2,1)} %param.9), channel_id=1, source_target_pairs={{0,2},{1,7},{2,4},{3,1},{4,6},{5,3},{6,0},{7,5},{8,10},{9,15},{10,... | collective-permute-start | bytes 3145736 | tf_op jit(solution)/shard_map/ppermute | solution.py:265
  3.9 29.5 %collective-permute-start = (bf16[2,64,4096]{2,1,0:T(8,128)(2,1)}, bf16[2,64,4096]{2,1,0:T(8,128)(2,1)S(1)}, u32[]{:S(2)}, u32[]{:S(2)}) collective-permute-start(bf16[2,64,4096]{2,1,0:T(8,128)(2,1)} %param.9), channel_id=1, source_target_pairs={{0,6},{1,3},{2,0},{3,5},{4,2},{5,7},{6,4},{7,1},{8,14},{9,11},{10,... | collective-permute-start | bytes 3145736 | tf_op jit(solution)/shard_map/ppermute | solution.py:265
  8.1 27.4 %copy-start.7 = (bf16[4096]{0:T(1024)(128)(2,1)S(1)}, bf16[4096]{0:T(1024)(128)(2,1)}, u32[]{:S(2)}) copy-start(bf16[4096]{0:T(1024)(128)(2,1)} %param.10) | copy-start | bytes 24580
  8.1 27.4 %copy-start.1 = (f32[2,512,2]{1,2,0:T(2,128)S(1)}, f32[2,512,2]{1,2,0:T(2,128)}, u32[]{:S(2)}) copy-start(f32[2,512,2]{1,2,0:T(2,128)} %param.13) | copy-start | bytes 24580
  8.1 27.4 %copy-start.2 = (f32[2,2]{1,0:T(2,128)S(1)}, f32[2,2]{1,0:T(2,128)}, u32[]{:S(2)}) copy-start(f32[2,2]{1,0:T(2,128)} %ng.1) | copy-start | bytes 52
  8.1 27.4 %copy-start.3 = (bf16[2,128]{1,0:T(2,128)(2,1)S(1)}, bf16[2,128]{1,0:T(2,128)(2,1)}, u32[]{:S(2)}) copy-start(bf16[2,128]{1,0:T(2,128)(2,1)} %q.1) | copy-start | bytes 1540
  8.1 27.4 %copy-start.4 = (bf16[2,128]{1,0:T(2,128)(2,1)S(1)}, bf16[2,128]{1,0:T(2,128)(2,1)}, u32[]{:S(2)}) copy-start(bf16[2,128]{1,0:T(2,128)(2,1)} %fk.1) | copy-start | bytes 1540
  8.1 27.4 %copy-start.5 = (bf16[2,128]{1,0:T(2,128)(2,1)S(1)}, bf16[2,128]{1,0:T(2,128)(2,1)}, u32[]{:S(2)}) copy-start(bf16[2,128]{1,0:T(2,128)(2,1)} %fv.1) | copy-start | bytes 1540
  8.1 27.7 %copy-start = (bf16[2,64,4096]{2,1,0:T(8,128)(2,1)S(1)}, bf16[2,64,4096]{2,1,0:T(8,128)(2,1)}, u32[]{:S(2)}) copy-start(bf16[2,64,4096]{2,1,0:T(8,128)(2,1)} %param.9) | copy-start | bytes 3145732
  8.4 27.4 %collective-permute-start.4 = (bf16[4096,256]{1,0:T(8,128)(2,1)S(1)}, bf16[4096,256]{1,0:T(8,128)(2,1)S(1)}, u32[]{:S(2)}, u32[]{:S(2)}) collective-permute-start(bf16[4096,256]{1,0:T(8,128)(2,1)S(1)} %constant_dynamic-update-slice_fusion.refs_2_.refs_4_.refs_5_), channel_id=1, source_target_pairs={{0,1},{1,0},{2,3},{3,2},{4,5},{5,4},{6,7},{7,6},{8,9},{9,8},{10,11... | collective-permute-start | bytes 6291464 | tf_op jit(solution)/shard_map/ppermute | solution.py:265
  27.9 16.9 %collective-permute-start.3 = (bf16[64,4096]{1,0:T(8,128)(2,1)S(1)}, bf16[64,4096]{1,0:T(8,128)(2,1)S(1)}, u32[]{:S(2)}, u32[]{:S(2)}) collective-permute-start(bf16[64,4096]{1,0:T(8,128)(2,1)S(1)} %slice_bitcast_fusion), channel_id=1, source_target_pairs={{0,2},{1,7},{2,4},{3,1},{4,6},{5,3},{6,0},{7,5},{8,10},{9,15},{10,... | collective-permute-start | bytes 1572872 | tf_op jit(solution)/shard_map/ppermute | solution.py:265
  33.5 12.7 %collective-permute-start.1 = (bf16[64,4096]{1,0:T(8,128)(2,1)S(1)}, bf16[64,4096]{1,0:T(8,128)(2,1)S(1)}, u32[]{:S(2)}, u32[]{:S(2)}) collective-permute-start(bf16[64,4096]{1,0:T(8,128)(2,1)S(1)} %slice_bitcast_fusion.1), channel_id=1, source_target_pairs={{0,6},{1,3},{2,0},{3,5},{4,2},{5,7},{6,4},{7,1},{8,14},{9,11},{10,... | collective-permute-start | bytes 1572872 | tf_op jit(solution)/shard_map/ppermute | solution.py:265
  39.9 9.4 %collective-permute-start.5 = (bf16[6,64,256]{2,1,0:T(8,128)(2,1)S(1)}, bf16[6,64,256]{2,1,0:T(8,128)(2,1)S(1)}, u32[]{:S(2)}, u32[]{:S(2)}) collective-permute-start(bf16[6,64,256]{2,1,0:T(8,128)(2,1)S(1)} %get-tuple-element.40), channel_id=1, source_target_pairs={{0,1},{1,0},{2,3},{3,2},{4,5},{5,4},{6,7},{7,6},{8,9},{9,8},{10,11... | collective-permute-start | bytes 589832 | tf_op jit(solution)/shard_map/ppermute | solution.py:265
